TPU v7x, 32 devices: a whole 2x2x4 slice. The times are simulated.
32 devices in a mesh: sp: 8 (over z, y), tp: 4 (over x, core).
Axes of the slice: x: 2, y: 2, z: 4, core: 2. Of those that a mesh axis runs over, the one named last changes fastest.
Arguments:
- queries_nope: bfloat16 [3072, 8, 128], P('sp', 'tp'), may hold values from -9 to 9
- queries_rope: bfloat16 [3072, 8, 64], P('sp', 'tp'), may hold values from -6 to 6
- latent: bfloat16 [3072, 512], P('sp'), may hold values from -8 to 8, as said below
- rope_key: bfloat16 [3072, 64], P('sp'), may hold values from -6 to 6
- latent_gain: float32 [512], replicated, may hold values from 0.1 to 1.9
- key_up: bfloat16 [512, 1024], P(None, 'tp'), may hold values from -0.25 to 0.25
- value_up: bfloat16 [512, 1024], P(None, 'tp'), may hold values from -0.25 to 0.25
- out_proj: bfloat16 [1024, 2048], P('tp'), may hold values from -0.75 to 0.75
- stream: bfloat16 [3072, 2048], P(('sp', 'tp')), may hold values from -6 to 6
- mix_gain: float32 [2048], replicated, may hold values from 0.1 to 1.9
- w_gate: bfloat16 [2048, 3072], P('sp', 'tp'), may hold values from -0.125 to 0.125
- w_up: bfloat16 [2048, 3072], P('sp', 'tp'), may hold values from -0.125 to 0.125
- w_down: bfloat16 [3072, 2048], P('tp', 'sp'), may hold values from -0.4375 to 0.4375
- mlp_gain: float32 [2048], replicated, may hold values from 0.1 to 1.9
Outputs:
- result: bfloat16 [3072, 2048], P(('sp', 'tp'))
Inputs may be any that keep to these rules, and one draw needn't show every extreme that they name: latent rows carry a mean vector that changes from one eighth of the sequence to the next.
All inputs are finite; a program needn't handle non-finite values.
Results may differ from a plain program's by a relative error of at most 0.017.
Values may be sent and summed in bfloat16 or wider, within the bound.
A program may use at most 192 MiB of HBM per device.

v0:
```python
import functools

import jax
import jax.numpy as jnp
from jax import lax
from jax.experimental import pallas as pl
from jax.experimental.pallas import tpu as pltpu
from jax.sharding import PartitionSpec as P

theta_base = 10000.0
residual_weight = 8.0**0.25
norm_floor = 1.0
big_negative = -1e30


def rotate(vector, first_row):
    half = vector.shape[-1] // 2
    rates = theta_base ** (-2.0 * jnp.arange(half, dtype=jnp.float32) / vector.shape[-1])
    places = (first_row + jnp.arange(vector.shape[0], dtype=jnp.int32)).astype(jnp.float32)
    angle = places[:, None] * rates[None, :]
    angle = angle.reshape((vector.shape[0],) + (1,) * (vector.ndim - 2) + (half,))
    cosine = jnp.cos(angle)
    sine = jnp.sin(angle)
    left = vector[..., :half]
    right = vector[..., half:]
    return jnp.concatenate([left * cosine - right * sine, left * sine + right * cosine], axis=-1)


def latent_norm(latent, latent_gain):
    wide = latent.astype(jnp.float32)
    factor = lax.rsqrt(jnp.mean(wide * wide, axis=-1, keepdims=True) + norm_floor)
    return (wide * factor * latent_gain).astype(jnp.bfloat16)


def layer_norm(values, gain):
    centre = jnp.mean(values, axis=-1, keepdims=True)
    centred = values - centre
    spread = jnp.mean(centred * centred, axis=-1, keepdims=True)
    return centred * lax.rsqrt(spread + norm_floor) * gain


mesh_id = pl.DeviceIdType.MESH
bf16 = jnp.bfloat16
f32 = jnp.float32


def layer_kernel(
    chain,
    teams,
    scale,
    qcat,
    latent_in,
    key_up,
    value_up,
    proj_in,
    stream,
    mix_gain,
    gate_in,
    up_in,
    down_in,
    mlp_gain,
    result,
    lat,
    gate,
    up,
    down,
    proj,
    heads_out,
    heads_in,
    rows,
    hidden,
    terms_out,
    mate_in,
    terms,
    arrived,
    wide,
    top,
    total,
    weighted,
    local_sem,
    lat_recv,
    lat_up,
    lat_side,
    lat_core,
    w_recv,
    w_side,
    w_up,
    w_down,
    proj_recv,
    proj_send,
    head_recv,
    head_send,
    row_recv,
    row_send,
    mate_recv,
    mate_send,
    term_recv,
    term_send,
):
    sp = lax.axis_index("sp")
    t = lax.axis_index("tp")
    q = sp // 2
    p = sp % 2
    other = 1 - p
    half = t % 2
    mate = t + 1 - 2 * half
    group = 2 * teams
    mine = half * teams + p * (teams // 2) + t // 2
    own_class = half * teams
    last = chain - 1
    head_count = qcat.shape[0]
    head_dim = value_up.shape[1] // head_count
    block_rows = qcat.shape[1]
    width = value_up.shape[0]
    has_up = q < last
    has_down = q > 0

    def place(pp, tt, qq=None):
        return ((q if qq is None else qq) * 2 + pp, tt)

    def remote(source, target, send, recv, device):
        return pltpu.make_async_remote_copy(
            src_ref=source,
            dst_ref=target,
            send_sem=send,
            recv_sem=recv,
            device_id=device,
            device_id_type=mesh_id,
        )

    barrier = pltpu.get_barrier_semaphore()
    place_here = p * teams + t
    for step in range(1, group):
        index = lax.rem(place_here + step, group)
        pl.semaphore_signal(
            barrier, inc=1, device_id=place(index // teams, index % teams), device_id_type=mesh_id
        )

    @pl.when(has_up)
    def _():
        pl.semaphore_signal(barrier, inc=1, device_id=place(p, t, q + 1), device_id_type=mesh_id)

    @pl.when(has_down)
    def _():
        pl.semaphore_signal(barrier, inc=1, device_id=place(p, t, q - 1), device_id_type=mesh_id)

    peers = group - 1 + jnp.where(has_up, 1, 0) + jnp.where(has_down, 1, 0)
    pl.semaphore_wait(barrier, peers)

    def lat_to_up(j, source):
        return remote(
            source, lat.at[j, p, half], lat_up.at[j], lat_recv.at[j, p, half], place(p, t, q + 1)
        )

    def lat_to_side(j, source):
        return remote(
            source, lat.at[j, p, half], lat_side.at[j], lat_recv.at[j, p, half], place(other, t)
        )

    def lat_to_core(j, pp):
        spot = lat.at[j, pp, half]
        return remote(spot, spot, lat_core.at[j, pp], lat_recv.at[j, pp, half], place(p, mate))

    def lat_wait(j, pp, hh):
        spot = lat.at[j, pp, hh]
        remote(spot, spot, lat_up.at[0], lat_recv.at[j, pp, hh], place(p, mate)).wait_recv()

    stores = (gate, up, down)
    hidden_half = gate.shape[3]

    def piece(w, which):
        start = pl.multiple_of(which * hidden_half, 128)
        if w == 0:
            return gate_in.at[:, pl.ds(start, hidden_half)]
        if w == 1:
            return up_in.at[:, pl.ds(start, hidden_half)]
        return down_in.at[pl.ds(start, hidden_half), :]

    def w_to_side(w):
        return remote(
            piece(w, other),
            stores[w].at[q, p],
            w_side.at[w],
            w_recv.at[w, q, p],
            place(other, t),
        )

    def w_to_up(w, j, pp):
        spot = stores[w].at[j, pp]
        return remote(spot, spot, w_up.at[w, j, pp], w_recv.at[w, j, pp], place(p, t, q + 1))

    def w_to_down(w, j, pp):
        spot = stores[w].at[j, pp]
        return remote(spot, spot, w_down.at[w, j, pp], w_recv.at[w, j, pp], place(p, t, q - 1))

    def w_wait(w, j, pp):
        spot = stores[w].at[j, pp]
        remote(spot, spot, w_up.at[w, 0, 0], w_recv.at[w, j, pp], place(p, mate)).wait_recv()

    def w_own(w):
        return pltpu.make_async_copy(piece(w, p), stores[w].at[q, p], local_sem.at[1 + w])

    own_lat = pltpu.make_async_copy(latent_in, lat.at[q, p], local_sem.at[0])
    own_proj = pltpu.make_async_copy(proj_in, proj.at[t], local_sem.at[4])

    def proj_to(step):
        tt = lax.rem(t + step, teams)
        return remote(proj_in, proj.at[t], proj_send.at[step], proj_recv.at[step], place(p, tt))

    def proj_mate():
        return remote(proj_in, proj.at[t], proj_send.at[1], proj_recv.at[1], place(p, mate))

    def proj_pass(step):
        spot = proj.at[lax.rem(t - step + teams, teams)]
        return remote(spot, spot, proj_send.at[step + 1], proj_recv.at[step + 1], place(p, mate))

    own_lat.start()
    w_own(0).start()
    w_own(1).start()
    w_own(2).start()

    @pl.when(has_up)
    def _():
        lat_to_up(q, latent_in.at[half]).start()

    lat_to_side(q, latent_in.at[half]).start()
    for w in range(3):
        w_to_side(w).start()
    own_proj.start()
    for step in range(2, teams, 2):
        proj_to(step).start()
    proj_mate().start()
    for w in range(3):
        w_own(w).wait()

        @pl.when(has_down)
        def _():
            w_to_down(w, q, p).start()

    top[...] = jnp.full_like(top, big_negative)
    total[...] = jnp.zeros_like(total)
    weighted[...] = jnp.zeros_like(weighted)

    def attend(j, pp, diagonal):
        block = lat[j, pp].reshape(block_rows, lat.shape[4])
        normed = block[:, :width]
        rotary = block[:, width:]
        keys = jnp.dot(normed, key_up[...], preferred_element_type=f32).astype(bf16)
        values = jnp.dot(normed, value_up[...], preferred_element_type=f32).astype(bf16)
        for h in range(head_count):
            span = slice(h * head_dim, (h + 1) * head_dim)
            both = jnp.concatenate([keys[:, span], rotary], axis=1)
            score = (
                lax.dot_general(
                    qcat[h], both, (((1,), (1,)), ((), ())), preferred_element_type=f32
                )
                * scale
            )
            if diagonal:
                across = lax.broadcasted_iota(jnp.int32, score.shape, 1)
                along = lax.broadcasted_iota(jnp.int32, score.shape, 0)
                score = jnp.where(across <= along, score, big_negative)
            old = top[h]
            new = jnp.maximum(old, jnp.max(score, axis=1, keepdims=True))
            powers = jnp.exp(score - new)
            shrink = jnp.exp(old - new)
            total[h] = total[h] * shrink + jnp.sum(powers, axis=1, keepdims=True)
            weighted[h] = weighted[h] * shrink + jnp.dot(
                powers.astype(bf16), values[:, span], preferred_element_type=f32
            )
            top[h] = new

    own_lat.wait()
    attend(q, p, True)

    for w in range(3):
        w_wait(w, q, other)

        @pl.when(has_down)
        def _():
            w_to_down(w, q, other).start()

    lat_wait(q, other, half)
    lat_to_core(q, other).start()

    def lat_step(s, carry):
        j = q - s

        @pl.when(j >= 0)
        def _():
            lat_wait(j, p, half)

            @pl.when(has_up)
            def _():
                lat_to_up(j, lat.at[j, p, half]).start()

            lat_to_side(j, lat.at[j, p, half]).start()
            lat_to_core(j, p).start()
            lat_wait(j, other, half)
            lat_to_core(j, other).start()

        return carry

    lax.fori_loop(1, chain, lat_step, 0)

    @pl.when(has_up)
    def _():
        for w in range(2):
            w_to_up(w, q, p).start()
            w_to_up(w, q, other).start()

    lat_wait(q, other, 1 - half)

    def whole_block(index, carry):
        j = q - (index + 1) // 2
        pp = jnp.where(index % 2 == 1, p, other)

        @pl.when(j >= 0)
        def _():
            @pl.when(index > 0)
            def _():
                lat_wait(j, pp, 1 - half)

            @pl.when((index > 0) | (p == 1))
            def _():
                attend(j, pp, False)

        return carry

    lax.fori_loop(0, 2 * chain - 1, whole_block, 0)

    part = block_rows // teams
    for h in range(head_count):
        span = slice(h * head_dim, (h + 1) * head_dim)
        done = (weighted[h] / total[h]).astype(bf16)
        heads_out[:, :, span] = done.reshape(teams, part, head_dim)

    def head_to(step):
        tt = lax.rem(t + step, teams)
        return remote(
            heads_out.at[tt], heads_in.at[t], head_send.at[step], head_recv.at[step], place(p, tt)
        )

    for step in range(1, teams):
        head_to(step).start()
    heads_in[t] = heads_out[t]

    def w_step(kinds, s):
        for w in kinds:
            for k in range(2):

                @pl.when(q - s >= 0)
                def _():
                    w_wait(w, q - s, k)

                    @pl.when(has_up)
                    def _():
                        w_to_up(w, q - s, k).start()

                @pl.when(q + s <= last)
                def _():
                    w_wait(w, q + s, k)

                    @pl.when(has_down)
                    def _():
                        w_to_down(w, q + s, k).start()

    def w_steps(kinds, first, end):
        def body(s, carry):
            w_step(kinds, s)
            return carry

        lax.fori_loop(first, end, body, 0)

    for step in range(2, teams, 2):
        proj_to(step).wait_recv()
        proj_pass(step).start()
    w_steps((0, 1), 1, 2)

    @pl.when(has_up)
    def _():
        w_to_up(2, q, p).start()
        w_to_up(2, q, other).start()

    own_proj.wait()
    proj_mate().wait_recv()
    for step in range(1, teams):
        head_to(step).wait_recv()
    for step in range(2, teams, 2):
        proj_pass(step).wait_recv()

    def project(k, carry):
        wide[...] += jnp.dot(heads_in[k], proj[k], preferred_element_type=f32)
        return carry

    wide[...] = residual_weight * stream[...].astype(f32)
    lax.fori_loop(0, teams, project, 0)
    rows[mine] = layer_norm(wide[...], mix_gain[...]).astype(bf16)

    stages = []
    bit = 2
    while bit < teams:
        stages.append(bit)
        bit *= 2
    stages += [0, 1]

    def flip(stage, pp, tt):
        if stage == 0:
            return 1 - pp, tt
        return pp, jnp.where((tt // stage) % 2 == 0, tt + stage, tt - stage)

    held = [(p, t)]
    for stage in stages:
        held = held + [flip(stage, pp, tt) for pp, tt in held]

    def row_copy(i, u):
        pp, tt = held[u]
        spot = rows.at[(tt % 2) * teams + pp * (teams // 2) + tt // 2]
        slot = 2**i - 1 + u
        partner = place(*flip(stages[i], p, t))
        return remote(spot, spot, row_send.at[slot], row_recv.at[slot], partner)

    for i in range(len(stages)):
        row_copy(i, 0).start()
    for i in range(len(stages)):
        for u in range(2**i):
            row_copy(i, u).wait_recv()
            for later in range(i + 1, len(stages)):
                row_copy(later, 2**i + u).start()
    w_steps((0, 1), 2, chain)

    def feed(k, carry):
        here = rows[pl.ds(2 * k, 2)].reshape(2 * part, rows.shape[2])
        gate_sum = jnp.dot(
            here, gate[...].reshape(-1, hidden_half), preferred_element_type=f32
        )
        up_sum = jnp.dot(here, up[...].reshape(-1, hidden_half), preferred_element_type=f32)
        value = gate_sum / (1.0 + jnp.exp(-gate_sum)) * up_sum
        hidden[pl.ds(2 * k, 2)] = value.astype(bf16).reshape(2, part, hidden_half)
        return carry

    lax.fori_loop(0, group // 2, feed, 0)

    my_turn = p * (teams // 2) + t // 2

    def term_mate(j):
        return remote(
            terms_out.at[j], mate_in.at[j], mate_send.at[j], mate_recv.at[j], place(p, mate)
        )

    def term_to(j, step):
        index = lax.rem(my_turn + step, teams)
        pp = index // (teams // 2)
        tt = 2 * (index % (teams // 2)) + half
        return remote(
            terms.at[j, index],
            arrived.at[j, my_turn],
            term_send.at[j, step],
            term_recv.at[j, step],
            place(pp, tt),
        )

    def lower(j):
        weights = jnp.concatenate([down[j, 0], down[j, 1]], axis=1)

        def product(first):
            here = hidden[pl.ds(first, teams)].reshape(teams * part, hidden_half)
            return jnp.dot(here, weights, preferred_element_type=f32)

        there = product(teams - own_class)
        terms_out[j] = there.astype(bf16).reshape(teams, part, there.shape[1])
        term_mate(j).start()
        kept = product(own_class)
        term_mate(j).wait_recv()
        kept = kept.reshape(teams, part, kept.shape[1]) + mate_in[j].astype(f32)
        terms[j] = kept.astype(bf16)
        for step in range(1, teams):
            term_to(j, step).start()

    lower(q)

    def lower_step(s, carry):
        w_step((2,), s)

        def one(side, inner):
            j = jnp.where(side == 0, q - s, q + s)

            @pl.when((j >= 0) & (j <= last))
            def _():
                lower(j)

            return inner

        lax.fori_loop(0, 2, one, 0)
        return carry

    lax.fori_loop(1, chain, lower_step, 0)

    def collect(j, carry):
        for step in range(1, teams):
            term_to(j, step).wait()
        return carry

    lax.fori_loop(0, chain, collect, 0)
    span_width = terms.shape[3]
    for j in range(chain):
        arrived[j, my_turn] = terms[j, my_turn]
        lowered = arrived[j, 0].astype(f32)
        for k in range(1, teams):
            lowered = lowered + arrived[j, k].astype(f32)
        span = slice(j * span_width, (j + 1) * span_width)
        wide[:, span] = residual_weight * rows[mine, :, span].astype(f32) + 0.5 * lowered
    result[...] = layer_norm(wide[...], mlp_gain[...]).astype(bf16)

    for w in range(3):
        w_to_side(w).wait_send()
    proj_mate().wait_send()
    for step in range(2, teams, 2):
        proj_to(step).wait_send()
        proj_pass(step).wait_send()
    for step in range(1, teams):
        head_to(step).wait_send()
    for i in range(len(stages)):
        for u in range(2**i):
            row_copy(i, u).wait_send()

    def drain(j, carry):
        term_mate(j).wait_send()

        @pl.when(has_up & (j <= q))
        def _():
            lat_to_up(j, lat.at[j, p, half]).wait_send()
            for w in range(3):
                for k in range(2):
                    w_to_up(w, j, k).wait_send()

        @pl.when(has_down & (j >= q))
        def _():
            for w in range(3):
                for k in range(2):
                    w_to_down(w, j, k).wait_send()

        @pl.when(j <= q)
        def _():
            lat_to_side(j, lat.at[j, p, half]).wait_send()
            lat_to_core(j, other).wait_send()

        @pl.when(j < q)
        def _():
            lat_to_core(j, p).wait_send()

        return carry

    lax.fori_loop(0, chain, drain, 0)


def per_device(
    chain,
    teams,
    queries_nope,
    queries_rope,
    latent,
    rope_key,
    latent_gain,
    key_up,
    value_up,
    out_proj,
    stream,
    mix_gain,
    w_gate,
    w_up,
    w_down,
    mlp_gain,
):
    row_count, head_count, head_dim = queries_nope.shape
    rope_dim = queries_rope.shape[2]
    first_row = lax.axis_index("sp") * row_count
    query_turned = rotate(queries_rope.astype(jnp.float32), first_row).astype(jnp.bfloat16)
    key_turned = rotate(rope_key.astype(jnp.float32), first_row).astype(jnp.bfloat16)
    normed = latent_norm(latent, latent_gain)
    scale = (head_dim + rope_dim) ** (-0.5)
    spare = -rope_dim % 128
    qcat = jnp.concatenate(
        [queries_nope, query_turned, jnp.zeros((row_count, head_count, spare), bf16)], axis=2
    ).transpose(1, 0, 2)
    latent_in = jnp.concatenate(
        [normed, key_turned, jnp.zeros((row_count, spare), bf16)], axis=1
    ).reshape(2, row_count // 2, -1)
    width = latent_in.shape[2]
    model, hidden_here = w_gate.shape[0] * 2 * chain, w_gate.shape[1]
    group = 2 * teams
    part = row_count // teams
    half_hidden = hidden_here // 2
    deep = w_gate.shape[0]
    slim = w_down.shape[1]
    stages = group - 1
    dma = pltpu.SemaphoreType.DMA
    vmem = pl.BlockSpec(memory_space=pltpu.VMEM)
    hbm = pl.BlockSpec(memory_space=pltpu.HBM)
    return pl.pallas_call(
        functools.partial(layer_kernel, chain, teams, scale),
        out_shape=jax.ShapeDtypeStruct((part, model), bf16),
        in_specs=[vmem, hbm, vmem, vmem, hbm, vmem, vmem, hbm, hbm, hbm, vmem],
        out_specs=vmem,
        scratch_shapes=[
            pltpu.VMEM((chain, 2, 2, row_count // 2, width), bf16),
            pltpu.VMEM((chain, 2, deep, half_hidden), bf16),
            pltpu.VMEM((chain, 2, deep, half_hidden), bf16),
            pltpu.VMEM((chain, 2, half_hidden, slim), bf16),
            pltpu.VMEM((teams,) + out_proj.shape, bf16),
            pltpu.VMEM((teams, part, head_count * head_dim), bf16),
            pltpu.VMEM((teams, part, head_count * head_dim), bf16),
            pltpu.VMEM((group, part, model), bf16),
            pltpu.VMEM((group, part, half_hidden), bf16),
            pltpu.VMEM((chain, teams, part, 2 * slim), bf16),
            pltpu.VMEM((chain, teams, part, 2 * slim), bf16),
            pltpu.VMEM((chain, teams, part, 2 * slim), bf16),
            pltpu.VMEM((chain, teams, part, 2 * slim), bf16),
            pltpu.VMEM((part, model), f32),
            pltpu.VMEM((head_count, row_count, 1), f32),
            pltpu.VMEM((head_count, row_count, 1), f32),
            pltpu.VMEM((head_count, row_count, head_dim), f32),
            dma((5,)),
            dma((chain, 2, 2)),
            dma((chain,)),
            dma((chain,)),
            dma((chain, 2)),
            dma((3, chain, 2)),
            dma((3,)),
            dma((3, chain, 2)),
            dma((3, chain, 2)),
            dma((teams,)),
            dma((teams,)),
            dma((teams,)),
            dma((teams,)),
            dma((stages,)),
            dma((stages,)),
            dma((chain,)),
            dma((chain,)),
            dma((chain, teams)),
            dma((chain, teams)),
        ],
        compiler_params=pltpu.CompilerParams(
            collective_id=0, has_side_effects=True, vmem_limit_bytes=60 * 1024 * 1024
        ),
    )(
        qcat,
        latent_in,
        key_up,
        value_up,
        out_proj,
        stream,
        mix_gain.reshape(1, -1),
        w_gate,
        w_up,
        w_down,
        mlp_gain.reshape(1, -1),
    )


def solution(mesh):
    return jax.shard_map(
        functools.partial(per_device, mesh.shape["sp"] // 2, mesh.shape["tp"]),
        mesh=mesh,
        in_specs=(
            P("sp", "tp", None),
            P("sp", "tp", None),
            P("sp", None),
            P("sp", None),
            P(),
            P(None, "tp"),
            P(None, "tp"),
            P("tp", None),
            P(("sp", "tp"), None),
            P(),
            P("sp", "tp"),
            P("sp", "tp"),
            P("tp", "sp"),
            P(),
        ),
        out_specs=P(("sp", "tp"), None),
        check_vma=False,
    )
```

profile of v0, /device:TPU:25, one launch (start us, length us, event | category | flops | bytes accessed | tf_op | source)
XLA Modules:
  0.0 133.2 jit_solution(17950661350035535588)
XLA Ops:
  0.0 0.8 convert_element_type.26
  0.8 0.3 subtract_convert_fusion.1
  1.1 0.1 copy.16
  1.2 0.0 copy-start.2
  1.2 0.1 copy.17
  1.4 0.8 copy-done.2
  2.1 0.2 copy.15
  2.3 0.0 copy-start.1
  2.4 0.2 subtract_convert_fusion
  2.6 0.1 pad.7.clone
  2.6 0.6 copy-done.1
  3.3 0.0 copy-start
  3.3 0.9 maximum_bitcast_fusion.qcat
  4.2 0.1 copy.19
  4.3 0.1 copy.20
  4.5 0.1 pad.3.clone
  4.5 0.0 copy-done
  4.5 0.2 fusion
  4.7 0.0 copy-start.3
  4.7 0.7 copy-done.3
  5.4 0.2 fusion.2
  5.6 0.9 maximum_maximum_fusion
  6.5 124.9 %shard_map.136 = bf16[96,2048]{1,0:T(8,128)(2,1)} custom-call(bf16[2,384,256]{2,1,0:T(8,128)(2,1)} %maximum_bitcast_fusion.qcat, bf16[2,192,640]{2,1,0:T(8,128)(2,1)} %bitcast.5, bf16[512,256]{1,0:T(8,128)(2,1)} %key_up.1, bf16[512,256]{1,0:T(8,128)(2,1)} %value_up.1, bf16[256,2048]{1,0:T(8,128)(2,1)} %proj_in.1, bf16[96,2048]{1,0:T(8,128)(2,1)} %stream.1, ...), custom_call_target="tpu_custom_call" | custom-call | tf_op jit(solution)/shard_map/pallas_call | solution.py:600
  131.4 1.8 %copy.22 = bf16[96,2048]{1,0:T(8,128)(2,1)} copy(bf16[96,2048]{1,0:T(8,128)(2,1)} %shard_map.136) | data formatting | bytes 786432
  (6 shorter events, 0.1 us)
Async XLA Ops:
  1.2 0.9 copy-start.2
  2.3 0.9 copy-start.1
  3.3 1.2 copy-start
  4.7 0.7 copy-start.3
where the time goes:
time: 134 us; the launch traced here: 133 us
  Pallas kernels  125 us (93%)
  local copies, waits for them, and re-layouts  4.67 us (3%)
  other arithmetic  3.45 us (3%)
    pallas_call x1, Pallas kernels, per_device(): pl.pallas_call(functools.partial(layer_kernel, chain, teams, scale), out_...  125 us
    unnamed x11, local copies, waits for them, and re-layouts  4.02 us

commit v1 on v0

v1 whole, which is shorter than its diff:
```python
import functools
import math

import jax
import jax.numpy as jnp
from jax import lax
from jax.experimental import pallas as pl
from jax.experimental.pallas import tpu as pltpu
from jax.sharding import PartitionSpec as P

theta_base = 10000.0
residual_weight = 8.0**0.25
norm_floor = 1.0
big_negative = -1e30


def rotate(vector, first_row):
    half = vector.shape[-1] // 2
    rates = theta_base ** (-2.0 * jnp.arange(half, dtype=jnp.float32) / vector.shape[-1])
    places = (first_row + jnp.arange(vector.shape[0], dtype=jnp.int32)).astype(jnp.float32)
    angle = places[:, None] * rates[None, :]
    angle = angle.reshape((vector.shape[0],) + (1,) * (vector.ndim - 2) + (half,))
    cosine = jnp.cos(angle)
    sine = jnp.sin(angle)
    left = vector[..., :half]
    right = vector[..., half:]
    return jnp.concatenate([left * cosine - right * sine, left * sine + right * cosine], axis=-1)


def latent_norm(latent, latent_gain):
    wide = latent.astype(jnp.float32)
    factor = lax.rsqrt(jnp.mean(wide * wide, axis=-1, keepdims=True) + norm_floor)
    return (wide * factor * latent_gain).astype(jnp.bfloat16)


def layer_norm(values, gain):
    centre = jnp.mean(values, axis=-1, keepdims=True)
    centred = values - centre
    spread = jnp.mean(centred * centred, axis=-1, keepdims=True)
    return centred * lax.rsqrt(spread + norm_floor) * gain


mesh_id = pl.DeviceIdType.MESH
bf16 = jnp.bfloat16
f32 = jnp.float32


def layer_kernel(
    chain,
    teams,
    scale,
    qcat,
    latent_in,
    key_up,
    value_up,
    proj_in,
    stream,
    mix_gain,
    gate_in,
    up_in,
    down_in,
    mlp_gain,
    result,
    lat,
    gate,
    up,
    down,
    proj,
    heads_out,
    heads_in,
    share_out,
    share_in,
    rows,
    hidden,
    terms_out,
    mate_in,
    terms,
    x_first,
    z_first,
    x_relay,
    z_relay,
    x_last,
    z_last,
    wide,
    top,
    total,
    weighted,
    local_sem,
    lat_recv,
    lat_z,
    lat_y,
    lat_w,
    lat_next,
    lat_x,
    lat_m,
    w_recv,
    w_z,
    w_y,
    core_recv,
    core_send,
    share_recv,
    share_send,
    row_recv,
    row_send,
    mate_recv,
    mate_send,
    term_recv,
    term_send,
):
    sp = lax.axis_index("sp")
    t = lax.axis_index("tp")
    q = sp // 2
    p = sp % 2
    other = 1 - p
    half = t % 2
    column = t // 2
    columns = teams // 2
    mate = t + 1 - 2 * half
    layer = q % 2
    group = 2 * teams
    mine = half * teams + column * 2 + layer
    last = chain - 1
    head_count = qcat.shape[0]
    head_dim = value_up.shape[1] // head_count
    block_rows = qcat.shape[1]
    width = value_up.shape[0]
    part = block_rows // teams

    def place(pp, tt, qq=None):
        return ((q if qq is None else qq) * 2 + pp, tt)

    def across(step):
        return lax.rem(t + step, teams)

    def remote(source, target, send, recv, device):
        return pltpu.make_async_remote_copy(
            src_ref=source,
            dst_ref=target,
            send_sem=send,
            recv_sem=recv,
            device_id=device,
            device_id_type=mesh_id,
        )

    def pair_place(zz, tt):
        return place(p, tt, q - layer + zz)

    far_steps = range(2, teams, 2)
    barrier = pltpu.get_barrier_semaphore()
    peers = [place(p, t, lax.rem(q + d, chain)) for d in range(1, chain)]
    peers += [place(other, t), place(p, mate)]
    peers += [place(p, across(step)) for step in far_steps]
    peers += [pair_place(1 - layer, across(step)) for step in far_steps]
    for device in peers:
        pl.semaphore_signal(barrier, inc=1, device_id=device, device_id_type=mesh_id)
    with jax.named_scope("barrier"):
        pl.semaphore_wait(barrier, len(peers))

    def lat_to_z(qq):
        return remote(
            latent_in.at[t], lat.at[q, p, t], lat_z.at[qq], lat_recv.at[q, p, t], place(p, t, qq)
        )

    def lat_to_next(j):
        spot = lat.at[j, p, t]
        return remote(spot, spot, lat_next.at[j], lat_recv.at[j, p, t], place(p, t, q + 1))

    def lat_side(j, step):
        spot = lat.at[j, p, across(step)]
        return remote(
            spot, spot, lat_w.at[j, step], lat_recv.at[j, p, across(step)], place(other, t)
        )

    def turned(j):
        return (j % 2 == 1) & (j < q)

    def lat_own_y():
        return remote(
            latent_in.at[t], lat.at[q, p, t], lat_y.at[q], lat_recv.at[q, p, t], place(other, t)
        )

    def lat_to_y(j):
        spot = lat.at[j, p, t]
        return remote(spot, spot, lat_y.at[j], lat_recv.at[j, p, t], place(other, t))

    def lat_to_x(j, pp, step):
        spot = lat.at[j, pp, t]
        return remote(
            spot, spot, lat_x.at[j, pp, step], lat_recv.at[j, pp, t], place(p, across(step))
        )

    def lat_to_m(j, pp, tt):
        spot = lat.at[j, pp, tt]
        return remote(spot, spot, lat_m.at[j, pp, tt], lat_recv.at[j, pp, tt], place(p, mate))

    def lat_wait(j, pp, tt):
        spot = lat.at[j, pp, tt]
        with jax.named_scope("lat_wait"):
            remote(spot, spot, lat_y.at[0], lat_recv.at[j, pp, tt], place(p, mate)).wait_recv()

    stores = (gate, up, down)
    hidden_half = gate.shape[3]

    def piece(w, which):
        start = pl.multiple_of(which * hidden_half, 128)
        if w == 0:
            return gate_in.at[:, pl.ds(start, hidden_half)]
        if w == 1:
            return up_in.at[:, pl.ds(start, hidden_half)]
        return down_in.at[pl.ds(start, hidden_half), :]

    def w_to_z(w, qq):
        return remote(
            piece(w, qq % 2),
            stores[w].at[q, p],
            w_z.at[w, qq],
            w_recv.at[w, q, p],
            place(p, t, qq),
        )

    def w_own_y(w):
        return remote(
            piece(w, layer), stores[w].at[q, p], w_y.at[w, q], w_recv.at[w, q, p], place(other, t)
        )

    def w_to_y(w, j):
        spot = stores[w].at[j, p]
        return remote(spot, spot, w_y.at[w, j], w_recv.at[w, j, p], place(other, t))

    def w_wait(w, j, pp):
        spot = stores[w].at[j, pp]
        with jax.named_scope("w_wait"):
            remote(spot, spot, w_y.at[w, 0], w_recv.at[w, j, pp], place(p, mate)).wait_recv()

    def w_own(w):
        return pltpu.make_async_copy(piece(w, layer), stores[w].at[q, p], local_sem.at[1 + w])

    own_lat = pltpu.make_async_copy(latent_in, lat.at[q, p], local_sem.at[0])
    own_proj = pltpu.make_async_copy(proj_in, proj.at[half], local_sem.at[4])
    proj_mate = remote(proj_in, proj.at[half], core_send.at[0], core_recv.at[0], place(p, mate))

    def lat_own_to_z(act):
        for d in range(1, chain):

            takes = (q + d <= last) & (((q + d) % 2 == 0) | ((d == 1) & (layer == 0)))

            @pl.when(takes)
            def _():
                act(lat_to_z(q + d))

    def toward(w, near, act):
        for d in (1,) if near else range(last, 1, -1):

            @pl.when((layer == 0) & (q + d <= last))
            def _():
                act(w_to_z(w, q + d))

            @pl.when((layer == 1) & (q - d >= 0))
            def _():
                act(w_to_z(w, q - d))

    def away(w, act):
        for d in range(last, 0, -1):

            @pl.when((layer == 1) & (q + d <= last))
            def _():
                act(w_to_z(w, q + d))

            @pl.when((layer == 0) & (q - d >= 0))
            def _():
                act(w_to_z(w, q - d))

    def start(copy):
        copy.start()

    def sent(copy):
        copy.wait_send()

    own_lat.start()
    lat_own_to_z(start)

    @pl.when(p == 0)
    def _():
        lat_own_y().start()

    w_own_y(0).start()
    patient = q == last - 1

    def all_toward():
        toward(0, True, start)
        toward(0, False, start)
        toward(1, False, start)
        toward(1, True, start)
        toward(2, True, start)

    for w in range(3):
        away(w, start)

    @pl.when(jnp.logical_not(patient))
    def _():
        all_toward()

    for w in range(3):
        w_own(w).start()
    own_proj.start()
    proj_mate.start()

    top[...] = jnp.full_like(top, big_negative)
    total[...] = jnp.zeros_like(total)
    weighted[...] = jnp.zeros_like(weighted)

    def attend(j, pp, diagonal):
        block = lat[j, pp].reshape(block_rows, lat.shape[4])
        normed = block[:, :width]
        rotary = block[:, width:]
        keys = jnp.dot(normed, key_up[...], preferred_element_type=f32).astype(bf16)
        values = jnp.dot(normed, value_up[...], preferred_element_type=f32).astype(bf16)
        for h in range(head_count):
            span = slice(h * head_dim, (h + 1) * head_dim)
            both = jnp.concatenate([keys[:, span], rotary], axis=1)
            score = lax.dot_general(
                qcat[h], both, (((1,), (1,)), ((), ())), preferred_element_type=f32
            )
            if diagonal:
                down_rows = lax.broadcasted_iota(jnp.int32, score.shape, 0)
                over_columns = lax.broadcasted_iota(jnp.int32, score.shape, 1)
                score = jnp.where(over_columns <= down_rows, score, big_negative)
            old = top[h]
            new = jnp.maximum(old, jnp.max(score, axis=1, keepdims=True))
            powers = jnp.exp2(score * scale - new * scale)
            shrink = jnp.exp2((old - new) * scale)
            total[h] = total[h] * shrink + jnp.sum(powers, axis=1, keepdims=True)
            weighted[h] = weighted[h] * shrink + jnp.dot(
                powers.astype(bf16), values[:, span], preferred_element_type=f32
            )
            top[h] = new

    with jax.named_scope("own_lat"):
        own_lat.wait()
    with jax.named_scope("attend_own"):
        attend(q, p, True)

    def is_edge(j):
        return (j % 4 == 0) | (j % 4 == 3)

    def forward(w, kind):
        for j in range(chain):
            distant = q // 2 != j // 2
            if kind == 1:
                takes = (q // 2 == j // 2) & (q != j)
            elif is_edge(j) == (kind == 0):
                takes = distant
            else:
                continue

            @pl.when(takes)
            def _():
                w_wait(w, j, p)
                w_to_y(w, j).start()

    def lat_step(s, carry):
        a = q - s

        @pl.when(a >= 0)
        def _():
            lat_wait(a, p, t)
            lat_to_y(a).start()
            for step in far_steps:
                lat_to_x(a, p, step).start()
            lat_to_m(a, p, t).start()

            @pl.when(layer == 0)
            def _():
                lat_to_next(a).start()

        b = q - s + 1

        @pl.when((b >= 0) & ((s >= 2) | (p == 1)))
        def _():
            lat_wait(b, other, t)

            @pl.when(jnp.logical_not(turned(b)))
            def _():
                for step in far_steps:
                    lat_to_x(b, other, step).start()

            lat_to_m(b, other, t).start()

        @pl.when(s == 3)
        def _():
            w_own_y(1).start()

        @pl.when((s == 3) & patient)
        def _():
            all_toward()

        def block(j, pp):
            for i in range(columns):
                lat_wait(j, pp, 2 * i + 1 - half)
            with jax.named_scope("attend"):
                attend(j, pp, False)

        def stage(k, inner):
            e = q - s + 2 + k

            @pl.when((e >= 0) & ((s >= 4) | ((s == 3) & ((k == 0) | (p == 1)))))
            def _():
                block(e, jnp.where(k == 0, p, other))

            c = b + k
            side = jnp.where(k == 0, p, other)
            ready = (s >= 2) & ((k == 0) | (s >= 3) | (p == 1))

            @pl.when((c >= 0) & ready)
            def _():
                for step in far_steps:
                    lat_wait(c, side, across(step))

                    @pl.when(turned(c) & (k == 0))
                    def _():
                        lat_side(c, step).start()

                    lat_to_m(c, side, across(step)).start()

            return inner

        lax.fori_loop(0, 2, stage, 0)
        for turn, w, kind in ((4, 0, 1), (5, 0, 0), (6, 1, 0)):

            @pl.when(s == turn)
            def _():
                forward(w, kind)

        return carry

    lax.fori_loop(1, max(chain + 3, 7), lat_step, 0)

    for h in range(head_count):
        span = slice(h * head_dim, (h + 1) * head_dim)
        done = (weighted[h] / total[h]).astype(bf16)
        done = done.reshape(teams, part, head_dim)
        for tt in range(teams):
            heads_out[tt % 2, tt // 2, :, span] = done[tt]

    heads_mate = remote(
        heads_out.at[1 - half], heads_in.at[half], core_send.at[1], core_recv.at[1], place(p, mate)
    )
    heads_mate.start()
    heads_in[half] = heads_out[half]
    own_proj.wait()
    for w in range(3):
        w_own(w).wait()
    with jax.named_scope("head_wait"):
        proj_mate.wait_recv()
        heads_mate.wait_recv()

    chunks = share_out.shape[0]
    span_share = share_out.shape[3]

    def project(i, c):
        span = slice(c * span_share, (c + 1) * span_share)
        return jnp.dot(
            heads_in[0, i], proj[0, :, span], preferred_element_type=f32
        ) + jnp.dot(heads_in[1, i], proj[1, :, span], preferred_element_type=f32)

    def share_to(c, step):
        i = lax.rem(column + step, columns)
        return remote(
            share_out.at[c, i],
            share_in.at[c, column],
            share_send.at[c, step],
            share_recv.at[c, step],
            place(p, 2 * i + half),
        )

    with jax.named_scope("project"):
        for c in range(chunks):
            for step in range(1, columns):
                i = lax.rem(column + step, columns)
                share_out[c, i] = project(i, c).astype(bf16)
                share_to(c, step).start()
        forward(1, 1)
        for c in range(chunks):
            span = slice(c * span_share, (c + 1) * span_share)
            wide[:, span] = residual_weight * stream[:, span].astype(f32) + project(column, c)
    for c in range(chunks):
        span = slice(c * span_share, (c + 1) * span_share)
        for step in range(1, columns):
            with jax.named_scope("share_wait"):
                share_to(c, step).wait_recv()
            source = lax.rem(column - step + columns, columns)
            wide[:, span] += share_in[c, source].astype(f32)
    with jax.named_scope("norm"):
        rows[mine] = layer_norm(wide[...], mix_gain[...]).astype(bf16)

    bits = []
    bit = 2
    while bit < teams:
        bits.append(bit)
        bit *= 2
    orders = (bits + [0, 1], [0] + bits + [1])
    depth = len(orders[0])
    sub = part // 2

    def flip(stage, zz, tt):
        if stage == 0:
            return 1 - zz, tt
        return zz, jnp.where((tt // stage) % 2 == 0, tt + stage, tt - stage)

    holdings = []
    for order in orders:
        held = [(layer, t)]
        for stage in order:
            held = held + [flip(stage, zz, tt) for zz, tt in held]
        holdings.append(held)

    def row_copy(o, i, u):
        zz, tt = holdings[o][u]
        index = (tt % 2) * teams + (tt // 2) * 2 + zz
        spot = rows.at[index, pl.ds(o * sub, sub)]
        slot = 2**i - 1 + u
        partner = pair_place(*flip(orders[o][i], layer, t))
        return remote(spot, spot, row_send.at[o, slot], row_recv.at[o, slot], partner)

    for i in range(depth):
        for o in range(2):
            row_copy(o, i, 0).start()
    forward(0, 2)
    forward(1, 2)
    w_own_y(2).start()
    forward(2, 1)
    def row_stage(i):
        for o in range(2):
            for u in range(2**i):
                with jax.named_scope("row_wait"):
                    row_copy(o, i, u).wait_recv()
                for later in range(i + 1, depth):
                    row_copy(o, later, 2**i + u).start()

    def feed(k, carry):
        here = rows[pl.ds(2 * k, 2)].reshape(2 * part, rows.shape[2])
        gate_sum = jnp.dot(
            here, gate[...].reshape(-1, hidden_half), preferred_element_type=f32
        )
        up_sum = jnp.dot(here, up[...].reshape(-1, hidden_half), preferred_element_type=f32)
        value = gate_sum / (1.0 + jnp.exp(-gate_sum)) * up_sum
        hidden[pl.ds(2 * k, 2)] = value.astype(bf16).reshape(2, part, hidden_half)
        return carry

    for i in range(depth - 1):
        row_stage(i)
        if i == 0:
            toward(2, False, start)
    for w in range(2):
        for j in range(chain):
            w_wait(w, j, other)
    with jax.named_scope("feed"):
        lax.fori_loop(half * columns, half * columns + columns, feed, 0)
    forward(2, 2)
    row_stage(depth - 1)
    with jax.named_scope("feed"):
        lax.fori_loop((1 - half) * columns, (1 - half) * columns + columns, feed, 0)

    def block_at(n):
        pair = lax.rem(q // 2 + n // 2, chain // 2)
        inner = 1 - pair % 2
        first = jnp.where(n < 2, layer, inner)
        return 2 * pair + jnp.where(n % 2 == 0, first, 1 - first)

    def term_mate(j):
        return remote(
            terms_out.at[j], mate_in.at[j], mate_send.at[j], mate_recv.at[j], place(p, mate)
        )

    def term_x(j, step):
        i = lax.rem(column + step, columns)
        return remote(
            terms.at[j, i, :, pl.ds(0, sub)],
            x_first.at[j, column],
            term_send.at[j, 0, step],
            term_recv.at[j, 0, step],
            place(p, 2 * i + half),
        )

    def term_z(j):
        return remote(
            terms.at[j, :, 1 - layer, pl.ds(sub, sub)],
            z_first.at[j],
            term_send.at[j, 1, 0],
            term_recv.at[j, 1, 0],
            pair_place(1 - layer, t),
        )

    def relay_x(j, step):
        i = lax.rem(column + step, columns)
        return remote(
            x_relay.at[j, i],
            x_last.at[j, column],
            term_send.at[j, 1, step],
            term_recv.at[j, 1, step],
            place(p, 2 * i + half),
        )

    def relay_z(j):
        return remote(
            z_relay.at[j],
            z_last.at[j],
            term_send.at[j, 0, 0],
            term_recv.at[j, 0, 0],
            pair_place(1 - layer, t),
        )

    def lower(j):
        weights = jnp.concatenate([down[j, 0], down[j, 1]], axis=1)
        own_rows = half * teams

        def product(first):
            here = hidden[pl.ds(first, teams)].reshape(teams * part, hidden_half)
            out = jnp.dot(here, weights, preferred_element_type=f32)
            return out.reshape(columns, 2, part, out.shape[1])

        terms_out[j] = product(teams - own_rows).astype(bf16)
        term_mate(j).start()
        kept = product(own_rows)
        with jax.named_scope("mate_wait"):
            term_mate(j).wait_recv()
        terms[j] = (kept + mate_in[j].astype(f32)).astype(bf16)
        for step in range(1, columns):
            term_x(j, step).start()
        term_z(j).start()

    def sources():
        return [lax.rem(column - step + columns, columns) for step in range(1, columns)]

    def relay(j):
        with jax.named_scope("relay_wait"):
            for step in range(1, columns):
                term_x(j, step).wait_recv()
            term_z(j).wait_recv()
        far = terms[j, column, 1 - layer, :sub].astype(f32)
        for source in sources():
            far = far + x_first[j, source, 1 - layer].astype(f32)
        z_relay[j] = far.astype(bf16)
        relay_z(j).start()
        for step in range(1, columns):
            i = lax.rem(column + step, columns)
            side = terms[j, i, layer, sub:].astype(f32) + z_first[j, i].astype(f32)
            x_relay[j, i] = side.astype(bf16)
            relay_x(j, step).start()

    def lower_step(n, carry):
        j = block_at(n)
        w_wait(2, j, other)
        with jax.named_scope("lower"):
            lower(j)

        @pl.when(n == 1)
        def _():
            forward(2, 0)

        @pl.when(n > 0)
        def _():
            relay(block_at(n - 1))

        return carry

    lax.fori_loop(0, chain, lower_step, 0)
    relay(block_at(chain - 1))
    span_width = terms.shape[4]
    for j in range(chain):
        with jax.named_scope("term_wait"):
            relay_z(j).wait_recv()
            for step in range(1, columns):
                relay_x(j, step).wait_recv()
        span = slice(j * span_width, (j + 1) * span_width)
        top_rows = terms[j, column, layer, :sub].astype(f32) + z_last[j].astype(f32)
        low_rows = terms[j, column, layer, sub:].astype(f32) + z_first[j, column].astype(f32)
        for source in sources():
            top_rows = top_rows + x_first[j, source, layer].astype(f32)
            low_rows = low_rows + x_last[j, source].astype(f32)
        kept_rows = residual_weight * rows[mine, :, span].astype(f32)
        wide[:sub, span] = kept_rows[:sub] + 0.5 * top_rows
        wide[sub:, span] = kept_rows[sub:] + 0.5 * low_rows
    with jax.named_scope("norm"):
        result[...] = layer_norm(wide[...], mlp_gain[...]).astype(bf16)

    proj_mate.wait_send()
    heads_mate.wait_send()
    for c in range(chunks):
        for step in range(1, columns):
            share_to(c, step).wait_send()
    for o in range(2):
        for i in range(depth):
            for u in range(2**i):
                row_copy(o, i, u).wait_send()

    @pl.when(p == 0)
    def _():
        lat_own_y().wait_send()

    for w in range(3):
        w_own_y(w).wait_send()

    def drain(j, carry):
        term_mate(j).wait_send()
        term_z(j).wait_send()
        relay_z(j).wait_send()
        for step in range(1, columns):
            term_x(j, step).wait_send()
            relay_x(j, step).wait_send()

        @pl.when(j != q)
        def _():
            for w in range(3):
                w_to_y(w, j).wait_send()

        @pl.when(j < q)
        def _():
            lat_to_y(j).wait_send()

            @pl.when(layer == 0)
            def _():
                lat_to_next(j).wait_send()

            for step in far_steps:
                lat_to_x(j, p, step).wait_send()

                @pl.when(turned(j))
                def _():
                    lat_side(j, step).wait_send()

            for i in range(columns):
                lat_to_m(j, p, 2 * i + half).wait_send()

        @pl.when((j < q) | ((j == q) & (p == 1)))
        def _():
            @pl.when(jnp.logical_not(turned(j)))
            def _():
                for step in far_steps:
                    lat_to_x(j, other, step).wait_send()

            for i in range(columns):
                lat_to_m(j, other, 2 * i + half).wait_send()

        return carry

    lax.fori_loop(0, chain, drain, 0)
    lat_own_to_z(sent)
    for w in range(3):
        toward(w, False, sent)
        toward(w, True, sent)
        away(w, sent)


def per_device(
    chain,
    teams,
    queries_nope,
    queries_rope,
    latent,
    rope_key,
    latent_gain,
    key_up,
    value_up,
    out_proj,
    stream,
    mix_gain,
    w_gate,
    w_up,
    w_down,
    mlp_gain,
):
    row_count, head_count, head_dim = queries_nope.shape
    rope_dim = queries_rope.shape[2]
    first_row = lax.axis_index("sp") * row_count
    query_turned = rotate(queries_rope.astype(jnp.float32), first_row).astype(jnp.bfloat16)
    key_turned = rotate(rope_key.astype(jnp.float32), first_row).astype(jnp.bfloat16)
    normed = latent_norm(latent, latent_gain)
    scale = (head_dim + rope_dim) ** (-0.5) * math.log2(math.e)
    spare = -rope_dim % 128
    qcat = jnp.concatenate(
        [queries_nope, query_turned, jnp.zeros((row_count, head_count, spare), bf16)], axis=2
    ).transpose(1, 0, 2)
    latent_in = jnp.concatenate(
        [normed, key_turned, jnp.zeros((row_count, spare), bf16)], axis=1
    ).reshape(teams, row_count // teams, -1)
    width = latent_in.shape[2]
    model, hidden_here = w_gate.shape[0] * 2 * chain, w_gate.shape[1]
    group = 2 * teams
    part = row_count // teams
    half_hidden = hidden_here // 2
    deep = w_gate.shape[0]
    slim = w_down.shape[1]
    stages = group - 1
    chunks = 4
    dma = pltpu.SemaphoreType.DMA
    vmem = pl.BlockSpec(memory_space=pltpu.VMEM)
    hbm = pl.BlockSpec(memory_space=pltpu.HBM)
    return pl.pallas_call(
        functools.partial(layer_kernel, chain, teams, scale),
        out_shape=jax.ShapeDtypeStruct((part, model), bf16),
        in_specs=[vmem, hbm, vmem, vmem, hbm, vmem, vmem, hbm, hbm, hbm, vmem],
        out_specs=vmem,
        scratch_shapes=[
            pltpu.VMEM((chain, 2, teams, part, width), bf16),
            pltpu.VMEM((chain, 2, deep, half_hidden), bf16),
            pltpu.VMEM((chain, 2, deep, half_hidden), bf16),
            pltpu.VMEM((chain, 2, half_hidden, slim), bf16),
            pltpu.VMEM((2,) + out_proj.shape, bf16),
            pltpu.VMEM((2, teams // 2, part, head_count * head_dim), bf16),
            pltpu.VMEM((2, teams // 2, part, head_count * head_dim), bf16),
            pltpu.VMEM((chunks, teams // 2, part, model // chunks), bf16),
            pltpu.VMEM((chunks, teams // 2, part, model // chunks), bf16),
            pltpu.VMEM((group, part, model), bf16),
            pltpu.VMEM((group, part, half_hidden), bf16),
            pltpu.VMEM((chain, teams // 2, 2, part, 2 * slim), bf16),
            pltpu.VMEM((chain, teams // 2, 2, part, 2 * slim), bf16),
            pltpu.VMEM((chain, teams // 2, 2, part, 2 * slim), bf16),
            pltpu.VMEM((chain, teams // 2, 2, part // 2, 2 * slim), bf16),
            pltpu.VMEM((chain, teams // 2, part // 2, 2 * slim), bf16),
            pltpu.VMEM((chain, teams // 2, part // 2, 2 * slim), bf16),
            pltpu.VMEM((chain, part // 2, 2 * slim), bf16),
            pltpu.VMEM((chain, teams // 2, part // 2, 2 * slim), bf16),
            pltpu.VMEM((chain, part // 2, 2 * slim), bf16),
            pltpu.VMEM((part, model), f32),
            pltpu.VMEM((head_count, row_count, 1), f32),
            pltpu.VMEM((head_count, row_count, 1), f32),
            pltpu.VMEM((head_count, row_count, head_dim), f32),
            dma((5,)),
            dma((chain, 2, teams)),
            dma((chain,)),
            dma((chain,)),
            dma((chain, teams)),
            dma((chain,)),
            dma((chain, 2, teams)),
            dma((chain, 2, teams)),
            dma((3, chain, 2)),
            dma((3, chain)),
            dma((3, chain)),
            dma((2,)),
            dma((2,)),
            dma((chunks, teams)),
            dma((chunks, teams)),
            dma((2, stages)),
            dma((2, stages)),
            dma((chain,)),
            dma((chain,)),
            dma((chain, 2, teams)),
            dma((chain, 2, teams)),
        ],
        compiler_params=pltpu.CompilerParams(
            collective_id=0, has_side_effects=True, vmem_limit_bytes=60 * 1024 * 1024
        ),
    )(
        qcat,
        latent_in,
        key_up,
        value_up,
        out_proj,
        stream,
        mix_gain.reshape(1, -1),
        w_gate,
        w_up,
        w_down,
        mlp_gain.reshape(1, -1),
    )


def solution(mesh):
    return jax.shard_map(
        functools.partial(per_device, mesh.shape["sp"] // 2, mesh.shape["tp"]),
        mesh=mesh,
        in_specs=(
            P("sp", "tp", None),
            P("sp", "tp", None),
            P("sp", None),
            P("sp", None),
            P(),
            P(None, "tp"),
            P(None, "tp"),
            P("tp", None),
            P(("sp", "tp"), None),
            P(),
            P("sp", "tp"),
            P("sp", "tp"),
            P("tp", "sp"),
            P(),
        ),
        out_specs=P(("sp", "tp"), None),
        check_vma=False,
    )
```

time: 134 us -> 106 us (0.79)
  the two profiles are of different devices: /device:TPU:25 before, /device:TPU:16 now
where the time goes in v1:
time: 106 us; the launch traced here: 105 us
  Pallas kernels  97.2 us (92%)
  local copies, waits for them, and re-layouts  4.67 us (4%)
  other arithmetic  3.45 us (3%)
    pallas_call x1, Pallas kernels, per_device(): pl.pallas_call(functools.partial(layer_kernel, chain, teams, scale), out_...  97.2 us
    unnamed x11, local copies, waits for them, and re-layouts  4.02 us

profile of v1, /device:TPU:16, one launch (start us, length us, event | category | flops | bytes accessed | tf_op | source)
XLA Modules:
  0.0 105.4 jit_solution(14053780152692059496)
XLA Ops:
  0.0 0.8 convert_element_type.26
  0.8 0.3 subtract_convert_fusion.1
  1.1 0.1 copy.16
  1.2 0.0 copy-start.2
  1.2 0.1 copy.17
  1.4 0.8 copy-done.2
  2.1 0.2 copy.15
  2.3 0.0 copy-start.1
  2.4 0.2 subtract_convert_fusion
  2.6 0.1 pad.7.clone
  2.6 0.6 copy-done.1
  3.3 0.0 copy-start
  3.3 0.9 maximum_bitcast_fusion.qcat
  4.2 0.1 copy.19
  4.3 0.1 copy.20
  4.5 0.1 pad.3.clone
  4.5 0.0 copy-done
  4.5 0.2 fusion
  4.7 0.0 copy-start.3
  4.7 0.7 copy-done.3
  5.4 0.2 fusion.2
  5.6 0.9 maximum_maximum_fusion
  6.5 97.2 %shard_map.136 = bf16[96,2048]{1,0:T(8,128)(2,1)} custom-call(bf16[2,384,256]{2,1,0:T(8,128)(2,1)} %maximum_bitcast_fusion.qcat, bf16[4,96,640]{2,1,0:T(8,128)(2,1)} %bitcast.5, bf16[512,256]{1,0:T(8,128)(2,1)} %key_up.1, bf16[512,256]{1,0:T(8,128)(2,1)} %value_up.1, bf16[256,2048]{1,0:T(8,128)(2,1)} %proj_in.1, bf16[96,2048]{1,0:T(8,128)(2,1)} %stream.1, ...), custom_call_target="tpu_custom_call" | custom-call | tf_op jit(solution)/shard_map/pallas_call | solution.py:799
  103.7 1.8 %copy.22 = bf16[96,2048]{1,0:T(8,128)(2,1)} copy(bf16[96,2048]{1,0:T(8,128)(2,1)} %shard_map.136) | data formatting | bytes 786432
  (6 shorter events, 0.1 us)
Async XLA Ops:
  1.2 0.9 copy-start.2
  2.3 0.9 copy-start.1
  3.3 1.2 %copy-start = (bf16[384,512]{1,0:T(8,128)(2,1)S(1)}, bf16[384,512]{1,0:T(8,128)(2,1)}, u32[]{:S(2)}) copy-start(bf16[384,512]{1,0:T(8,128)(2,1)} %param.16) | copy-start | bytes 1179652
  4.7 0.7 copy-start.3

commit v2 on v1

--- a/solution.py
+++ b/solution.py
@@ -3,6 +3,7 @@
 
 import jax
 import jax.numpy as jnp
+import numpy as np
 from jax import lax
 from jax.experimental import pallas as pl
 from jax.experimental.pallas import tpu as pltpu
@@ -12,19 +13,6 @@
 residual_weight = 8.0**0.25
 norm_floor = 1.0
 big_negative = -1e30
-
-
-def rotate(vector, first_row):
-    half = vector.shape[-1] // 2
-    rates = theta_base ** (-2.0 * jnp.arange(half, dtype=jnp.float32) / vector.shape[-1])
-    places = (first_row + jnp.arange(vector.shape[0], dtype=jnp.int32)).astype(jnp.float32)
-    angle = places[:, None] * rates[None, :]
-    angle = angle.reshape((vector.shape[0],) + (1,) * (vector.ndim - 2) + (half,))
-    cosine = jnp.cos(angle)
-    sine = jnp.sin(angle)
-    left = vector[..., :half]
-    right = vector[..., half:]
-    return jnp.concatenate([left * cosine - right * sine, left * sine + right * cosine], axis=-1)
 
 
 def latent_norm(latent, latent_gain):
@@ -49,18 +37,35 @@
     chain,
     teams,
     scale,
-    qcat,
-    latent_in,
-    key_up,
-    value_up,
+    rope_dim,
+    nope_hbm,
+    rope_hbm,
+    latent_hbm,
+    rope_key_hbm,
+    latent_gain_hbm,
+    rates_hbm,
+    key_up_hbm,
+    value_up_hbm,
     proj_in,
-    stream,
-    mix_gain,
+    stream_hbm,
+    mix_gain_hbm,
     gate_in,
     up_in,
     down_in,
+    mlp_gain_hbm,
+    result,
+    nope,
+    rope,
+    latent_in,
+    rope_key,
+    latent_gain,
+    rates,
+    key_up,
+    value_up,
+    stream,
+    mix_gain,
     mlp_gain,
-    result,
+    qcat,
     lat,
     gate,
     up,
@@ -85,6 +90,7 @@
     top,
     total,
     weighted,
+    load_sem,
     local_sem,
     lat_recv,
     lat_z,
@@ -153,12 +159,31 @@
     peers += [pair_place(1 - layer, across(step)) for step in far_steps]
     for device in peers:
         pl.semaphore_signal(barrier, inc=1, device_id=device, device_id_type=mesh_id)
-    with jax.named_scope("barrier"):
-        pl.semaphore_wait(barrier, len(peers))
+
+    loads = [
+        pltpu.make_async_copy(source, target, load_sem.at[i])
+        for i, (source, target) in enumerate(
+            (
+                (latent_hbm, latent_in),
+                (rope_key_hbm, rope_key),
+                (latent_gain_hbm, latent_gain),
+                (rates_hbm, rates),
+                (rope_hbm, rope),
+                (nope_hbm, nope),
+                (key_up_hbm, key_up),
+                (value_up_hbm, value_up),
+                (stream_hbm, stream),
+                (mix_gain_hbm, mix_gain),
+                (mlp_gain_hbm, mlp_gain),
+            )
+        )
+    ]
+    for load in loads:
+        load.start()
 
     def lat_to_z(qq):
         return remote(
-            latent_in.at[t], lat.at[q, p, t], lat_z.at[qq], lat_recv.at[q, p, t], place(p, t, qq)
+            lat.at[q, p, t], lat.at[q, p, t], lat_z.at[qq], lat_recv.at[q, p, t], place(p, t, qq)
         )
 
     def lat_to_next(j):
@@ -168,7 +193,7 @@
     def lat_side(j, step):
         spot = lat.at[j, p, across(step)]
         return remote(
-            spot, spot, lat_w.at[j, step], lat_recv.at[j, p, across(step)], place(other, t)
+            spot, spot, lat_w.at[j, step // 2 - 1], lat_recv.at[j, p, across(step)], place(other, t)
         )
 
     def turned(j):
@@ -176,7 +201,7 @@
 
     def lat_own_y():
         return remote(
-            latent_in.at[t], lat.at[q, p, t], lat_y.at[q], lat_recv.at[q, p, t], place(other, t)
+            lat.at[q, p, t], lat.at[q, p, t], lat_y.at[q], lat_recv.at[q, p, t], place(other, t)
         )
 
     def lat_to_y(j):
@@ -186,12 +211,12 @@
     def lat_to_x(j, pp, step):
         spot = lat.at[j, pp, t]
         return remote(
-            spot, spot, lat_x.at[j, pp, step], lat_recv.at[j, pp, t], place(p, across(step))
+            spot, spot, lat_x.at[j, pp, step // 2 - 1], lat_recv.at[j, pp, t], place(p, across(step))
         )
 
     def lat_to_m(j, pp, tt):
         spot = lat.at[j, pp, tt]
-        return remote(spot, spot, lat_m.at[j, pp, tt], lat_recv.at[j, pp, tt], place(p, mate))
+        return remote(spot, spot, lat_m.at[j, pp, tt // 2], lat_recv.at[j, pp, tt], place(p, mate))
 
     def lat_wait(j, pp, tt):
         spot = lat.at[j, pp, tt]
@@ -235,10 +260,11 @@
     def w_own(w):
         return pltpu.make_async_copy(piece(w, layer), stores[w].at[q, p], local_sem.at[1 + w])
 
-    own_lat = pltpu.make_async_copy(latent_in, lat.at[q, p], local_sem.at[0])
     own_proj = pltpu.make_async_copy(proj_in, proj.at[half], local_sem.at[4])
     proj_mate = remote(proj_in, proj.at[half], core_send.at[0], core_recv.at[0], place(p, mate))
 
+    beyond = range(2, chain)
+
     def lat_own_to_z(act):
         for d in range(1, chain):
 
@@ -249,7 +275,7 @@
                 act(lat_to_z(q + d))
 
     def toward(w, near, act):
-        for d in (1,) if near else range(last, 1, -1):
+        for d in (1,) if near else range(2, chain) if w == 2 else range(last, 1, -1):
 
             @pl.when((layer == 0) & (q + d <= last))
             def _():
@@ -259,8 +285,8 @@
             def _():
                 act(w_to_z(w, q - d))
 
-    def away(w, act):
-        for d in range(last, 0, -1):
+    def away(w, distances, act):
+        for d in distances:
 
             @pl.when((layer == 1) & (q + d <= last))
             def _():
@@ -276,7 +302,40 @@
     def sent(copy):
         copy.wait_send()
 
-    own_lat.start()
+    for w in range(3):
+        w_own(w).start()
+    own_proj.start()
+
+    lanes = head_count * rope_dim
+    turn_rows = lax.broadcasted_iota(jnp.int32, (block_rows, lanes), 0)
+    turn_lanes = lax.broadcasted_iota(jnp.int32, (block_rows, lanes), 1)
+    left = lax.rem(turn_lanes, rope_dim) < rope_dim // 2
+    loads[3].wait()
+    with jax.named_scope("angles"):
+        angle = (sp * block_rows + turn_rows).astype(f32) * rates[...]
+        cosine = jnp.cos(angle)
+        sine = jnp.sin(angle)
+        sine = jnp.where(left, -sine, sine)
+
+    def turn(vector):
+        ahead = pltpu.roll(vector, lanes - rope_dim // 2, 1)
+        behind = pltpu.roll(vector, rope_dim // 2, 1)
+        return vector * cosine + jnp.where(left, ahead, behind) * sine
+
+    def alone(vector):
+        return jnp.where(turn_lanes < rope_dim, vector, 0.0).astype(bf16)
+
+    for load in loads[:3]:
+        load.wait()
+    with jax.named_scope("latent"):
+        lat[q, p, :, :, :width] = latent_norm(latent_in[...], latent_gain[...]).reshape(
+            teams, part, width
+        )
+        key = rope_key[...].astype(f32)
+        key = turn(jnp.concatenate([key] * head_count, axis=0).T)
+        lat[q, p, :, :, width:] = alone(key).reshape(teams, part, lanes)
+    with jax.named_scope("barrier"):
+        pl.semaphore_wait(barrier, len(peers))
     lat_own_to_z(start)
 
     @pl.when(p == 0)
@@ -288,22 +347,38 @@
 
     def all_toward():
         toward(0, True, start)
+
+        @pl.when(layer == 0)
+        def _():
+            toward(1, True, start)
+
+            @pl.when(jnp.logical_not(patient))
+            def _():
+                toward(2, True, start)
+
         toward(0, False, start)
         toward(1, False, start)
-        toward(1, True, start)
-        toward(2, True, start)
-
-    for w in range(3):
-        away(w, start)
+
+        @pl.when(layer == 1)
+        def _():
+            toward(1, True, start)
+            toward(2, True, start)
+
+    for w, distances in ((0, (1,)), (1, (1,)), (0, beyond), (1, beyond), (2, (1,))):
+        away(w, distances, start)
 
     @pl.when(jnp.logical_not(patient))
     def _():
         all_toward()
 
-    for w in range(3):
-        w_own(w).start()
-    own_proj.start()
     proj_mate.start()
+    for load in loads[4:6]:
+        load.wait()
+    turned_queries = turn(rope[...].astype(f32).T)
+    for h in range(head_count):
+        qcat[h, :, :head_dim] = nope[:, h * head_dim : (h + 1) * head_dim]
+        shifted = turned_queries if h == 0 else pltpu.roll(turned_queries, lanes - h * rope_dim, 1)
+        qcat[h, :, head_dim:] = alone(shifted)
 
     top[...] = jnp.full_like(top, big_negative)
     total[...] = jnp.zeros_like(total)
@@ -335,10 +410,12 @@
             )
             top[h] = new
 
-    with jax.named_scope("own_lat"):
-        own_lat.wait()
+    for load in loads[6:]:
+        load.wait()
     with jax.named_scope("attend_own"):
         attend(q, p, True)
+
+    own = "own"
 
     def is_edge(j):
         return (j % 4 == 0) | (j % 4 == 3)
@@ -358,6 +435,33 @@
                 w_wait(w, j, p)
                 w_to_y(w, j).start()
 
+    plans = {
+        "early": (((0, 1),), ((0, 2), (0, 1)), ((0, 1),), ()),
+        "late": (((0, 0), (1, 1)), ((0, 0), (1, 1)), ((0, 2),), (own,)),
+        "after": ((), (), ((1, 2), own), ((0, 0),)),
+        "share": (((1, 0), own, (2, 1)), ((1, 0),), ((1, 1),), ((0, 1),)),
+        "half": ((), (), (), ((1, 0), (1, 1))),
+        "rows": ((), ((1, 2), own, (2, 1)), ((0, 0), (1, 0)), ((0, 2), (1, 2))),
+        "near": (((0, 2),), (), ((2, 1),), ()),
+        "middle": (((1, 2),), (), (), ()),
+        "far": ((), (), ((2, 2),), ()),
+        "last": (((2, 2),), ((2, 2),), ((2, 0),), ((2, 0),)),
+        "end": ((), ((2, 0),), (), ((2, 2),)),
+        "loop": (((2, 0),), (), (), ((2, 1),)),
+    }
+
+    def pass_along(name):
+        for kind_of, plan in enumerate(plans[name]):
+            if plan:
+
+                @pl.when(q % 4 == kind_of)
+                def _():
+                    for entry in plan:
+                        if entry is own:
+                            w_own_y(2).start()
+                        else:
+                            forward(*entry)
+
     def lat_step(s, carry):
         a = q - s
 
@@ -425,15 +529,17 @@
             return inner
 
         lax.fori_loop(0, 2, stage, 0)
-        for turn, w, kind in ((4, 0, 1), (5, 0, 0), (6, 1, 0)):
+        for turn, name in ((4, "early"), (5, "late")):
 
             @pl.when(s == turn)
             def _():
-                forward(w, kind)
+                pass_along(name)
 
         return carry
 
-    lax.fori_loop(1, max(chain + 3, 7), lat_step, 0)
+    lax.fori_loop(1, max(chain + 3, 6), lat_step, 0)
+    pass_along("after")
+
 
     for h in range(head_count):
         span = slice(h * head_dim, (h + 1) * head_dim)
@@ -468,8 +574,8 @@
         return remote(
             share_out.at[c, i],
             share_in.at[c, column],
-            share_send.at[c, step],
-            share_recv.at[c, step],
+            share_send.at[c, step - 1],
+            share_recv.at[c, step - 1],
             place(p, 2 * i + half),
         )
 
@@ -479,7 +585,7 @@
                 i = lax.rem(column + step, columns)
                 share_out[c, i] = project(i, c).astype(bf16)
                 share_to(c, step).start()
-        forward(1, 1)
+        pass_along("share")
         for c in range(chunks):
             span = slice(c * span_share, (c + 1) * span_share)
             wide[:, span] = residual_weight * stream[:, span].astype(f32) + project(column, c)
@@ -490,6 +596,8 @@
                 share_to(c, step).wait_recv()
             source = lax.rem(column - step + columns, columns)
             wide[:, span] += share_in[c, source].astype(f32)
+        if c == 1:
+            pass_along("half")
     with jax.named_scope("norm"):
         rows[mine] = layer_norm(wide[...], mix_gain[...]).astype(bf16)
 
@@ -525,10 +633,7 @@
     for i in range(depth):
         for o in range(2):
             row_copy(o, i, 0).start()
-    forward(0, 2)
-    forward(1, 2)
-    w_own_y(2).start()
-    forward(2, 1)
+    pass_along("rows")
     def row_stage(i):
         for o in range(2):
             for u in range(2**i):
@@ -550,22 +655,103 @@
     for i in range(depth - 1):
         row_stage(i)
         if i == 0:
+            pass_along("near")
+
             toward(2, False, start)
+
+            @pl.when(patient)
+            def _():
+                toward(2, True, start)
+
+            @pl.when(layer == 0)
+            def _():
+                away(2, beyond, start)
+
+            pass_along("middle")
+
+    @pl.when(layer == 1)
+    def _():
+        away(2, beyond, start)
+
+    pass_along("far")
     for w in range(2):
         for j in range(chain):
             w_wait(w, j, other)
     with jax.named_scope("feed"):
         lax.fori_loop(half * columns, half * columns + columns, feed, 0)
-    forward(2, 2)
+    pass_along("last")
     row_stage(depth - 1)
     with jax.named_scope("feed"):
         lax.fori_loop((1 - half) * columns, (1 - half) * columns + columns, feed, 0)
 
+    def settle(j, carry):
+        @pl.when(j != q)
+        def _():
+            for w in range(2):
+                w_to_y(w, j).wait_send()
+
+        @pl.when(j < q)
+        def _():
+            lat_to_y(j).wait_send()
+
+            @pl.when(layer == 0)
+            def _():
+                lat_to_next(j).wait_send()
+
+            for step in far_steps:
+                lat_to_x(j, p, step).wait_send()
+
+                @pl.when(turned(j))
+                def _():
+                    lat_side(j, step).wait_send()
+
+            for i in range(columns):
+                lat_to_m(j, p, 2 * i + half).wait_send()
+
+        @pl.when((j < q) | ((j == q) & (p == 1)))
+        def _():
+            @pl.when(jnp.logical_not(turned(j)))
+            def _():
+                for step in far_steps:
+                    lat_to_x(j, other, step).wait_send()
+
+            for i in range(columns):
+                lat_to_m(j, other, 2 * i + half).wait_send()
+
+        return carry
+
+    with jax.named_scope("settle"):
+        proj_mate.wait_send()
+        heads_mate.wait_send()
+        for c in range(chunks):
+            for step in range(1, columns):
+                share_to(c, step).wait_send()
+
+        @pl.when(p == 0)
+        def _():
+            lat_own_y().wait_send()
+
+        lax.fori_loop(0, chain, settle, 0)
+        lat_own_to_z(sent)
+        for w in range(2):
+            w_own_y(w).wait_send()
+            toward(w, False, sent)
+            toward(w, True, sent)
+            away(w, range(1, chain), sent)
+    pass_along("end")
+
     def block_at(n):
-        pair = lax.rem(q // 2 + n // 2, chain // 2)
-        inner = 1 - pair % 2
-        first = jnp.where(n < 2, layer, inner)
-        return 2 * pair + jnp.where(n % 2 == 0, first, 1 - first)
+        here = q // 2
+        upper = here % 2
+        skip = 2 - upper
+        ahead = jnp.maximum(n - skip, 0)
+        there = lax.rem(here + 1 + ahead // 2, chain // 2)
+        edge = 2 * there + there % 2
+        distant = jnp.where((ahead + upper) % 2 == 1, edge, 4 * there + 1 - edge)
+        own_edge = 2 * here + upper
+        own_inner = 4 * here + 1 - own_edge
+        chosen = jnp.where(n == 0, own_edge, jnp.where(n < skip, own_inner, distant))
+        return jnp.where((upper == 1) & (n == chain - 1), own_inner, chosen)
 
     def term_mate(j):
         return remote(
@@ -610,18 +796,20 @@
             pair_place(1 - layer, t),
         )
 
-    def lower(j):
+    own_rows = half * teams
+
+    def product(j, first):
         weights = jnp.concatenate([down[j, 0], down[j, 1]], axis=1)
-        own_rows = half * teams
-
-        def product(first):
-            here = hidden[pl.ds(first, teams)].reshape(teams * part, hidden_half)
-            out = jnp.dot(here, weights, preferred_element_type=f32)
-            return out.reshape(columns, 2, part, out.shape[1])
-
-        terms_out[j] = product(teams - own_rows).astype(bf16)
+        here = hidden[pl.ds(first, teams)].reshape(teams * part, hidden_half)
+        out = jnp.dot(here, weights, preferred_element_type=f32)
+        return out.reshape(columns, 2, part, out.shape[1])
+
+    def lower_mate(j):
+        terms_out[j] = product(j, teams - own_rows).astype(bf16)
         term_mate(j).start()
-        kept = product(own_rows)
+
+    def lower_own(j):
+        kept = product(j, own_rows)
         with jax.named_scope("mate_wait"):
             term_mate(j).wait_recv()
         terms[j] = (kept + mate_in[j].astype(f32)).astype(bf16)
@@ -649,23 +837,29 @@
             relay_x(j, step).start()
 
     def lower_step(n, carry):
-        j = block_at(n)
-        w_wait(2, j, other)
-        with jax.named_scope("lower"):
-            lower(j)
+        @pl.when(n < chain)
+        def _():
+            j = block_at(n)
+            w_wait(2, j, other)
+            with jax.named_scope("lower_mate"):
+                lower_mate(j)
+
+        @pl.when((n >= 1) & (n <= chain))
+        def _():
+            with jax.named_scope("lower_own"):
+                lower_own(block_at(n - 1))
 
         @pl.when(n == 1)
         def _():
-            forward(2, 0)
-
-        @pl.when(n > 0)
-        def _():
-            relay(block_at(n - 1))
+            pass_along("loop")
+
+        @pl.when(n >= 3)
+        def _():
+            relay(block_at(n - 3))
 
         return carry
 
-    lax.fori_loop(0, chain, lower_step, 0)
-    relay(block_at(chain - 1))
+    lax.fori_loop(0, chain + 3, lower_step, 0)
     span_width = terms.shape[4]
     for j in range(chain):
         with jax.named_scope("term_wait"):
@@ -684,22 +878,14 @@
     with jax.named_scope("norm"):
         result[...] = layer_norm(wide[...], mlp_gain[...]).astype(bf16)
 
-    proj_mate.wait_send()
-    heads_mate.wait_send()
-    for c in range(chunks):
-        for step in range(1, columns):
-            share_to(c, step).wait_send()
     for o in range(2):
         for i in range(depth):
             for u in range(2**i):
                 row_copy(o, i, u).wait_send()
-
-    @pl.when(p == 0)
-    def _():
-        lat_own_y().wait_send()
-
-    for w in range(3):
-        w_own_y(w).wait_send()
+    w_own_y(2).wait_send()
+    toward(2, False, sent)
+    toward(2, True, sent)
+    away(2, range(1, chain), sent)
 
     def drain(j, carry):
         term_mate(j).wait_send()
@@ -711,45 +897,12 @@
 
         @pl.when(j != q)
         def _():
-            for w in range(3):
-                w_to_y(w, j).wait_send()
-
-        @pl.when(j < q)
-        def _():
-            lat_to_y(j).wait_send()
-
-            @pl.when(layer == 0)
-            def _():
-                lat_to_next(j).wait_send()
-
-            for step in far_steps:
-                lat_to_x(j, p, step).wait_send()
-
-                @pl.when(turned(j))
-                def _():
-                    lat_side(j, step).wait_send()
-
-            for i in range(columns):
-                lat_to_m(j, p, 2 * i + half).wait_send()
-
-        @pl.when((j < q) | ((j == q) & (p == 1)))
-        def _():
-            @pl.when(jnp.logical_not(turned(j)))
-            def _():
-                for step in far_steps:
-                    lat_to_x(j, other, step).wait_send()
-
-            for i in range(columns):
-                lat_to_m(j, other, 2 * i + half).wait_send()
+            w_to_y(2, j).wait_send()
 
         return carry
 
-    lax.fori_loop(0, chain, drain, 0)
-    lat_own_to_z(sent)
-    for w in range(3):
-        toward(w, False, sent)
-        toward(w, True, sent)
-        away(w, sent)
+    with jax.named_scope("drain"):
+        lax.fori_loop(0, chain, drain, 0)
 
 
 def per_device(
@@ -772,19 +925,13 @@
 ):
     row_count, head_count, head_dim = queries_nope.shape
     rope_dim = queries_rope.shape[2]
-    first_row = lax.axis_index("sp") * row_count
-    query_turned = rotate(queries_rope.astype(jnp.float32), first_row).astype(jnp.bfloat16)
-    key_turned = rotate(rope_key.astype(jnp.float32), first_row).astype(jnp.bfloat16)
-    normed = latent_norm(latent, latent_gain)
     scale = (head_dim + rope_dim) ** (-0.5) * math.log2(math.e)
-    spare = -rope_dim % 128
-    qcat = jnp.concatenate(
-        [queries_nope, query_turned, jnp.zeros((row_count, head_count, spare), bf16)], axis=2
-    ).transpose(1, 0, 2)
-    latent_in = jnp.concatenate(
-        [normed, key_turned, jnp.zeros((row_count, spare), bf16)], axis=1
-    ).reshape(teams, row_count // teams, -1)
-    width = latent_in.shape[2]
+    lanes = head_count * rope_dim
+    half_rope = rope_dim // 2
+    rates = theta_base ** (-2.0 * (np.arange(lanes) % half_rope) / rope_dim)
+    rates = jnp.asarray(rates, f32).reshape(1, lanes)
+    rank = latent.shape[1]
+    width = rank + lanes
     model, hidden_here = w_gate.shape[0] * 2 * chain, w_gate.shape[1]
     group = 2 * teams
     part = row_count // teams
@@ -797,11 +944,23 @@
     vmem = pl.BlockSpec(memory_space=pltpu.VMEM)
     hbm = pl.BlockSpec(memory_space=pltpu.HBM)
     return pl.pallas_call(
-        functools.partial(layer_kernel, chain, teams, scale),
-        out_shape=jax.ShapeDtypeStruct((part, model), bf16),
-        in_specs=[vmem, hbm, vmem, vmem, hbm, vmem, vmem, hbm, hbm, hbm, vmem],
+        functools.partial(layer_kernel, chain, teams, scale, rope_dim),
+        out_shape=pltpu.VMEM((part, model), bf16),
+        in_specs=[hbm] * 15,
         out_specs=vmem,
         scratch_shapes=[
+            pltpu.VMEM((row_count, head_count * head_dim), bf16),
+            pltpu.VMEM((lanes, row_count), bf16),
+            pltpu.VMEM((row_count, rank), bf16),
+            pltpu.VMEM((rope_dim, row_count), bf16),
+            pltpu.VMEM((1, rank), f32),
+            pltpu.VMEM((1, lanes), f32),
+            pltpu.VMEM(key_up.shape, bf16),
+            pltpu.VMEM(value_up.shape, bf16),
+            pltpu.VMEM((part, model), bf16),
+            pltpu.VMEM((1, model), f32),
+            pltpu.VMEM((1, model), f32),
+            pltpu.VMEM((head_count, row_count, head_dim + lanes), bf16),
             pltpu.VMEM((chain, 2, teams, part, width), bf16),
             pltpu.VMEM((chain, 2, deep, half_hidden), bf16),
             pltpu.VMEM((chain, 2, deep, half_hidden), bf16),
@@ -826,34 +985,39 @@
             pltpu.VMEM((head_count, row_count, 1), f32),
             pltpu.VMEM((head_count, row_count, 1), f32),
             pltpu.VMEM((head_count, row_count, head_dim), f32),
+            dma((11,)),
             dma((5,)),
             dma((chain, 2, teams)),
             dma((chain,)),
             dma((chain,)),
-            dma((chain, teams)),
+            dma((chain, teams // 2 - 1)),
             dma((chain,)),
-            dma((chain, 2, teams)),
-            dma((chain, 2, teams)),
+            dma((chain, 2, teams // 2 - 1)),
+            dma((chain, 2, teams // 2)),
             dma((3, chain, 2)),
             dma((3, chain)),
             dma((3, chain)),
             dma((2,)),
             dma((2,)),
-            dma((chunks, teams)),
-            dma((chunks, teams)),
+            dma((chunks, teams // 2 - 1)),
+            dma((chunks, teams // 2 - 1)),
             dma((2, stages)),
             dma((2, stages)),
             dma((chain,)),
             dma((chain,)),
-            dma((chain, 2, teams)),
-            dma((chain, 2, teams)),
+            dma((chain, 2, teams // 2)),
+            dma((chain, 2, teams // 2)),
         ],
         compiler_params=pltpu.CompilerParams(
             collective_id=0, has_side_effects=True, vmem_limit_bytes=60 * 1024 * 1024
         ),
     )(
-        qcat,
-        latent_in,
+        queries_nope.reshape(row_count, head_count * head_dim),
+        queries_rope.transpose(1, 2, 0).reshape(lanes, row_count),
+        latent,
+        rope_key.T,
+        latent_gain.reshape(1, -1),
+        rates,
         key_up,
         value_up,
         out_proj,

time: 106 us -> 92.8 us (0.88)
  Pallas kernels: 97.2 us -> 90.3 us
  other arithmetic: 3.45 us -> 0 us
  local copies, waits for them, and re-layouts: 4.67 us -> 2.38 us
    pallas_call x1, Pallas kernels: 97.2 us -> 90.3 us  [per_device(): pl.pallas_call(functools.partial(layer_kernel, chain, teams, scale, rope_...]
    unnamed x11 -> x2, local copies, waits for them, and re-layouts: 4.02 us -> 2.38 us
where the time goes in v2:
time: 92.8 us; the launch traced here: 92.7 us
  Pallas kernels  90.3 us (97%)
  local copies, waits for them, and re-layouts  2.38 us (3%)
    pallas_call x1, Pallas kernels, per_device(): pl.pallas_call(functools.partial(layer_kernel, chain, teams, scale, rope_...  90.3 us
    unnamed x2, local copies, waits for them, and re-layouts  2.38 us

profile of v2, /device:TPU:16, one launch (start us, length us, event | category | flops | bytes accessed | tf_op | source)
XLA Modules:
  0.0 92.7 jit_solution(14111152306605315485)
XLA Ops:
  0.0 1.6 %copy.18 = bf16[48,8,2,128]{3,1,2,0:T(8,128)(2,1)} copy(bf16[48,8,2,128]{3,2,1,0:T(2,128)(2,1)} %bitcast.12) | data formatting | bytes 393216
  1.6 90.3 %shard_map.145 = bf16[96,2048]{1,0:T(8,128)(2,1)S(1)} custom-call(bf16[384,256]{1,0:T(8,128)(2,1)} %bitcast.11, bf16[128,384]{1,0:T(8,128)(2,1)} %bitcast.13, bf16[384,512]{1,0:T(8,128)(2,1)} %latent_hbm.1, bf16[64,384]{1,0:T(8,128)(2,1)} %bitcast.14, f32[1,512]{1,0:T(1,128)} %bitcast.17, f32[1,128]{1,0:T(1,128)} %constant.5.rates_hbm, ...), custom_call_target="tpu_custom_call" | custom-call | tf_op jit(solution)/shard_map/pallas_call | solution.py:946
  91.9 0.7 copy.20

commit v3 on v2

--- a/solution.py
+++ b/solution.py
@@ -66,6 +66,7 @@
     mix_gain,
     mlp_gain,
     qcat,
+    value_turned,
     lat,
     gate,
     up,
@@ -86,6 +87,7 @@
     z_relay,
     x_last,
     z_last,
+    lowered,
     wide,
     top,
     total,
@@ -364,7 +366,7 @@
             toward(1, True, start)
             toward(2, True, start)
 
-    for w, distances in ((0, (1,)), (1, (1,)), (0, beyond), (1, beyond), (2, (1,))):
+    for w, distances in ((0, (1,)), (0, beyond), (1, (1,)), (1, beyond), (2, (1,))):
         away(w, distances, start)
 
     @pl.when(jnp.logical_not(patient))
@@ -374,9 +376,10 @@
     proj_mate.start()
     for load in loads[4:6]:
         load.wait()
+    nope_wide = nope[...].astype(f32)
     turned_queries = turn(rope[...].astype(f32).T)
     for h in range(head_count):
-        qcat[h, :, :head_dim] = nope[:, h * head_dim : (h + 1) * head_dim]
+        qcat[h, :, :head_dim] = nope_wide[:, h, :].astype(bf16)
         shifted = turned_queries if h == 0 else pltpu.roll(turned_queries, lanes - h * rope_dim, 1)
         qcat[h, :, head_dim:] = alone(shifted)
 
@@ -389,29 +392,32 @@
         normed = block[:, :width]
         rotary = block[:, width:]
         keys = jnp.dot(normed, key_up[...], preferred_element_type=f32).astype(bf16)
-        values = jnp.dot(normed, value_up[...], preferred_element_type=f32).astype(bf16)
+        values = lax.dot_general(
+            value_turned[...], normed, (((1,), (1,)), ((), ())), preferred_element_type=f32
+        ).astype(bf16)
         for h in range(head_count):
             span = slice(h * head_dim, (h + 1) * head_dim)
             both = jnp.concatenate([keys[:, span], rotary], axis=1)
             score = lax.dot_general(
-                qcat[h], both, (((1,), (1,)), ((), ())), preferred_element_type=f32
+                both, qcat[h], (((1,), (1,)), ((), ())), preferred_element_type=f32
             )
             if diagonal:
-                down_rows = lax.broadcasted_iota(jnp.int32, score.shape, 0)
-                over_columns = lax.broadcasted_iota(jnp.int32, score.shape, 1)
-                score = jnp.where(over_columns <= down_rows, score, big_negative)
+                source_rows = lax.broadcasted_iota(jnp.int32, score.shape, 0)
+                query_rows = lax.broadcasted_iota(jnp.int32, score.shape, 1)
+                score = jnp.where(source_rows <= query_rows, score, big_negative)
             old = top[h]
-            new = jnp.maximum(old, jnp.max(score, axis=1, keepdims=True))
+            new = jnp.maximum(old, jnp.max(score, axis=0, keepdims=True))
             powers = jnp.exp2(score * scale - new * scale)
             shrink = jnp.exp2((old - new) * scale)
-            total[h] = total[h] * shrink + jnp.sum(powers, axis=1, keepdims=True)
+            total[h] = total[h] * shrink + jnp.sum(powers, axis=0, keepdims=True)
             weighted[h] = weighted[h] * shrink + jnp.dot(
-                powers.astype(bf16), values[:, span], preferred_element_type=f32
+                values[span], powers.astype(bf16), preferred_element_type=f32
             )
             top[h] = new
 
     for load in loads[6:]:
         load.wait()
+    value_turned[...] = value_up[...].astype(f32).T.astype(bf16)
     with jax.named_scope("attend_own"):
         attend(q, p, True)
 
@@ -437,17 +443,18 @@
 
     plans = {
         "early": (((0, 1),), ((0, 2), (0, 1)), ((0, 1),), ()),
-        "late": (((0, 0), (1, 1)), ((0, 0), (1, 1)), ((0, 2),), (own,)),
-        "after": ((), (), ((1, 2), own), ((0, 0),)),
+        "late": (((0, 0), (1, 1)), ((0, 0), (1, 1)), ((0, 2),), ((0, 2),)),
+        "after": ((), (), (own,), ((0, 0),)),
         "share": (((1, 0), own, (2, 1)), ((1, 0),), ((1, 1),), ((0, 1),)),
         "half": ((), (), (), ((1, 0), (1, 1))),
-        "rows": ((), ((1, 2), own, (2, 1)), ((0, 0), (1, 0)), ((0, 2), (1, 2))),
+        "rows": ((), ((1, 2), own, (2, 1)), ((0, 0), (1, 0), (1, 2)), ((1, 2), own)),
         "near": (((0, 2),), (), ((2, 1),), ()),
         "middle": (((1, 2),), (), (), ()),
         "far": ((), (), ((2, 2),), ()),
-        "last": (((2, 2),), ((2, 2),), ((2, 0),), ((2, 0),)),
-        "end": ((), ((2, 0),), (), ((2, 2),)),
-        "loop": (((2, 0),), (), (), ((2, 1),)),
+        "last": (((2, 2),), ((2, 2),), ((2, 0),), ()),
+        "end": ((), (), (), ((2, 0),)),
+        "first": ((), (), (), ((2, 2), (2, 1))),
+        "second": (((2, 0),), ((2, 0),), (), ()),
     }
 
     def pass_along(name):
@@ -543,7 +550,7 @@
 
     for h in range(head_count):
         span = slice(h * head_dim, (h + 1) * head_dim)
-        done = (weighted[h] / total[h]).astype(bf16)
+        done = (weighted[h] / total[h]).T.astype(bf16)
         done = done.reshape(teams, part, head_dim)
         for tt in range(teams):
             heads_out[tt % 2, tt // 2, :, span] = done[tt]
@@ -596,7 +603,7 @@
                 share_to(c, step).wait_recv()
             source = lax.rem(column - step + columns, columns)
             wide[:, span] += share_in[c, source].astype(f32)
-        if c == 1:
+        if c == 0:
             pass_along("half")
     with jax.named_scope("norm"):
         rows[mine] = layer_norm(wide[...], mix_gain[...]).astype(bf16)
@@ -668,21 +675,22 @@
                 away(2, beyond, start)
 
             pass_along("middle")
-
-    @pl.when(layer == 1)
-    def _():
-        away(2, beyond, start)
-
     pass_along("far")
     for w in range(2):
         for j in range(chain):
             w_wait(w, j, other)
     with jax.named_scope("feed"):
         lax.fori_loop(half * columns, half * columns + columns, feed, 0)
+
+    @pl.when(layer == 1)
+    def _():
+        away(2, beyond, start)
+
     pass_along("last")
     row_stage(depth - 1)
     with jax.named_scope("feed"):
         lax.fori_loop((1 - half) * columns, (1 - half) * columns + columns, feed, 0)
+    pass_along("end")
 
     def settle(j, carry):
         @pl.when(j != q)
@@ -738,7 +746,6 @@
             toward(w, False, sent)
             toward(w, True, sent)
             away(w, range(1, chain), sent)
-    pass_along("end")
 
     def block_at(n):
         here = q // 2
@@ -836,45 +843,52 @@
             x_relay[j, i] = side.astype(bf16)
             relay_x(j, step).start()
 
-    def lower_step(n, carry):
-        @pl.when(n < chain)
-        def _():
-            j = block_at(n)
-            w_wait(2, j, other)
-            with jax.named_scope("lower_mate"):
-                lower_mate(j)
-
-        @pl.when((n >= 1) & (n <= chain))
-        def _():
-            with jax.named_scope("lower_own"):
-                lower_own(block_at(n - 1))
-
-        @pl.when(n == 1)
-        def _():
-            pass_along("loop")
-
-        @pl.when(n >= 3)
-        def _():
-            relay(block_at(n - 3))
-
-        return carry
-
-    lax.fori_loop(0, chain + 3, lower_step, 0)
     span_width = terms.shape[4]
-    for j in range(chain):
+
+    def finish(j):
         with jax.named_scope("term_wait"):
             relay_z(j).wait_recv()
             for step in range(1, columns):
                 relay_x(j, step).wait_recv()
-        span = slice(j * span_width, (j + 1) * span_width)
         top_rows = terms[j, column, layer, :sub].astype(f32) + z_last[j].astype(f32)
         low_rows = terms[j, column, layer, sub:].astype(f32) + z_first[j, column].astype(f32)
         for source in sources():
             top_rows = top_rows + x_first[j, source, layer].astype(f32)
             low_rows = low_rows + x_last[j, source].astype(f32)
+        lowered[j, :sub] = top_rows
+        lowered[j, sub:] = low_rows
+
+    def lower_step(n, carry):
+        @pl.when(n < chain)
+        def _():
+            j = block_at(n)
+            w_wait(2, j, other)
+            with jax.named_scope("lower_mate"):
+                lower_mate(j)
+            with jax.named_scope("lower_own"):
+                lower_own(j)
+
+        for turn, name in ((0, "first"), (1, "second")):
+
+            @pl.when(n == turn)
+            def _():
+                pass_along(name)
+
+        @pl.when((n >= 1) & (n <= chain))
+        def _():
+            relay(block_at(n - 1))
+
+        @pl.when(n >= 2)
+        def _():
+            finish(block_at(n - 2))
+
+        return carry
+
+    lax.fori_loop(0, chain + 2, lower_step, 0)
+    for j in range(chain):
+        span = slice(j * span_width, (j + 1) * span_width)
         kept_rows = residual_weight * rows[mine, :, span].astype(f32)
-        wide[:sub, span] = kept_rows[:sub] + 0.5 * top_rows
-        wide[sub:, span] = kept_rows[sub:] + 0.5 * low_rows
+        wide[:, span] = kept_rows + 0.5 * lowered[j]
     with jax.named_scope("norm"):
         result[...] = layer_norm(wide[...], mlp_gain[...]).astype(bf16)
 
@@ -949,7 +963,7 @@
         in_specs=[hbm] * 15,
         out_specs=vmem,
         scratch_shapes=[
-            pltpu.VMEM((row_count, head_count * head_dim), bf16),
+            pltpu.VMEM(queries_nope.shape, bf16),
             pltpu.VMEM((lanes, row_count), bf16),
             pltpu.VMEM((row_count, rank), bf16),
             pltpu.VMEM((rope_dim, row_count), bf16),
@@ -961,6 +975,7 @@
             pltpu.VMEM((1, model), f32),
             pltpu.VMEM((1, model), f32),
             pltpu.VMEM((head_count, row_count, head_dim + lanes), bf16),
+            pltpu.VMEM((value_up.shape[1], value_up.shape[0]), bf16),
             pltpu.VMEM((chain, 2, teams, part, width), bf16),
             pltpu.VMEM((chain, 2, deep, half_hidden), bf16),
             pltpu.VMEM((chain, 2, deep, half_hidden), bf16),
@@ -981,10 +996,11 @@
             pltpu.VMEM((chain, part // 2, 2 * slim), bf16),
             pltpu.VMEM((chain, teams // 2, part // 2, 2 * slim), bf16),
             pltpu.VMEM((chain, part // 2, 2 * slim), bf16),
+            pltpu.VMEM((chain, part, 2 * slim), f32),
             pltpu.VMEM((part, model), f32),
-            pltpu.VMEM((head_count, row_count, 1), f32),
-            pltpu.VMEM((head_count, row_count, 1), f32),
-            pltpu.VMEM((head_count, row_count, head_dim), f32),
+            pltpu.VMEM((head_count, 1, row_count), f32),
+            pltpu.VMEM((head_count, 1, row_count), f32),
+            pltpu.VMEM((head_count, head_dim, row_count), f32),
             dma((11,)),
             dma((5,)),
             dma((chain, 2, teams)),
@@ -1012,7 +1028,7 @@
             collective_id=0, has_side_effects=True, vmem_limit_bytes=60 * 1024 * 1024
         ),
     )(
-        queries_nope.reshape(row_count, head_count * head_dim),
+        queries_nope,
         queries_rope.transpose(1, 2, 0).reshape(lanes, row_count),
         latent,
         rope_key.T,

time: 92.8 us -> 89.1 us (0.960)
  Pallas kernels: 90.3 us -> 87.9 us
  local copies, waits for them, and re-layouts: 2.38 us -> 0.75 us
    pallas_call x1, Pallas kernels: 90.3 us -> 87.9 us  [per_device(): pl.pallas_call(functools.partial(layer_kernel, chain, teams, scale, rope_...]
    unnamed x2 -> x1, local copies, waits for them, and re-layouts: 2.38 us -> 0.75 us
where the time goes in v3:
time: 89.1 us; the launch traced here: 88.7 us
  Pallas kernels  87.9 us (99%)
    pallas_call x1, Pallas kernels, per_device(): pl.pallas_call(functools.partial(layer_kernel, chain, teams, scale, rope_...  87.9 us

profile of v3, /device:TPU:16, one launch (start us, length us, event | category | flops | bytes accessed | tf_op | source)
XLA Modules:
  0.0 88.7 jit_solution(3471156201223364144)
XLA Ops:
  0.0 87.9 %shard_map.145 = bf16[96,2048]{1,0:T(8,128)(2,1)S(1)} custom-call(bf16[384,2,128]{2,1,0:T(2,128)(2,1)} %nope_hbm.1, bf16[128,384]{1,0:T(8,128)(2,1)} %bitcast.7, bf16[384,512]{1,0:T(8,128)(2,1)} %latent_hbm.1, bf16[64,384]{1,0:T(8,128)(2,1)} %bitcast.8, f32[1,512]{1,0:T(1,128)} %bitcast.11, f32[1,128]{1,0:T(1,128)} %constant.5.rates_hbm, ...), custom_call_target="tpu_custom_call" | custom-call | tf_op jit(solution)/shard_map/pallas_call | solution.py:960
  87.9 0.7 copy.17
